TPU v7x, 32 devices: a whole 2x2x4 slice. The times are simulated.
32 devices in a mesh: sp: 8 (over z, x), dp: 4 (over y, core).
Axes of the slice: x: 2, y: 2, z: 4, core: 2. Of those that a mesh axis runs over, the one named last changes fastest.
Arguments:
- tokens: bfloat16 [4, 4096, 2048], P('dp', 'sp'), may hold values from -6 to 6
- segments: int32 [4, 4096], P('dp', 'sp'), may hold values from 0 to 3, never falling along the last dimension, each value on 1 to 2048 neighbouring positions
- w_lin: bfloat16 [2048, 1024], P('dp'), may hold values from -0.125 to 0.125
- w_gate: bfloat16 [2048, 1024], P('dp'), may hold values from -0.125 to 0.125
- w_out: bfloat16 [1024, 2048], P(None, 'dp'), may hold values from -0.1875 to 0.1875
- conv_kernel: float32 [31, 1024], replicated, may hold values from -1 to 1
- conv_bias: float32 [1024], replicated, may hold values from -3 to 3
- norm_gain: float32 [1024], replicated, may hold values from 0.1 to 1.9
- norm_bias: float32 [1024], replicated, may hold values from -3 to 3
Outputs:
- mixed_out: bfloat16 [4, 4096, 2048], P('dp', 'sp')
Inputs may be any that keep to these rules, and one draw needn't show every extreme that they name: `segments`: within each sequence document numbers never fall; a document is a run of equal numbers of at most four times 512 positions.
All inputs are finite; a program needn't handle non-finite values.
Results may differ from a plain program's by a relative error of at most 0.0062.
Values may be sent and summed in bfloat16 or wider, within the bound.
A program may use at most 64 MiB of HBM per device.

v0:
```python
import jax
import jax.numpy as jnp
from jax import lax
from jax.sharding import PartitionSpec as P

K = 31


def from_behind(value, axis, by):
    devices = lax.axis_size(axis)
    pairs = [(i, i + by) for i in range(devices) if 0 <= i + by < devices]
    return lax.ppermute(value, axis, pairs)


def conv_doc(values, doc_ids, kernel, bias):
    taps = kernel.shape[0]
    reach = taps - 1
    length = values.shape[1]
    place = lax.iota(jnp.int32, length)
    change = jnp.concatenate([jnp.ones((1,), jnp.bool_), doc_ids[1:] != doc_ids[:-1]])
    begins = lax.cummax(jnp.where(change, place, 0), axis=0)[reach:]
    here = place[reach:]
    total = bias[:, None] + kernel[reach][:, None] * values[:, reach:].astype(jnp.float32)
    for back in range(1, taps):
        piece = values[:, reach - back : length - back].astype(jnp.float32)
        keep = here - back >= begins
        total = total + kernel[reach - back][:, None] * jnp.where(keep[None, :], piece, 0.0)
    return total


def body(tokens, segments, w_lin, w_gate, w_out, conv_kernel, conv_bias, norm_gain, norm_bias):
    rows = tokens[0]
    doc_ids = segments[0]
    count = rows.shape[0]
    reach = K - 1
    first = jnp.einsum(
        "rc,tr->ct",
        lax.all_gather(w_lin, "dp", axis=0, tiled=True),
        rows,
        preferred_element_type=jnp.float32,
    )
    second = jnp.einsum(
        "rc,tr->ct",
        lax.all_gather(w_gate, "dp", axis=0, tiled=True),
        rows,
        preferred_element_type=jnp.float32,
    )
    glu = (first * jax.nn.sigmoid(second)).astype(jnp.bfloat16)
    tail, tail_ids = from_behind((glu[:, count - reach :], doc_ids[count - reach :]), "sp", 1)
    extended = jnp.concatenate([tail, glu], axis=1)
    ext_ids = jnp.concatenate([tail_ids, doc_ids], axis=0)
    conv = conv_doc(extended, ext_ids, conv_kernel, conv_bias)
    conved = lax.optimization_barrier(conv.astype(jnp.bfloat16))
    values = conved.astype(jnp.float32)
    mean = jnp.mean(values, axis=0, keepdims=True)
    var = jnp.mean(jnp.square(values - mean), axis=0, keepdims=True)
    normed = (values - mean) * lax.rsqrt(var + 1e-05) * norm_gain[:, None] + norm_bias[:, None]
    act = jax.nn.silu(normed).astype(jnp.bfloat16)
    mixed_out = jnp.einsum(
        "ct,cr->tr",
        act,
        lax.all_gather(w_out, "dp", axis=1, tiled=True),
        preferred_element_type=jnp.float32,
    ).astype(jnp.bfloat16)
    return mixed_out[None]


def solution(mesh):
    placed = (
        P("dp", "sp", None),
        P("dp", "sp"),
        P("dp", None),
        P("dp", None),
        P(None, "dp"),
        P(),
        P(),
        P(),
        P(),
    )
    return jax.shard_map(
        body, mesh=mesh, in_specs=placed, out_specs=P("dp", "sp", None), check_vma=False
    )
```

profile of v0, /device:TPU:0, one launch (start us, length us, event | category | flops | bytes accessed | tf_op | source)
XLA Modules:
  0.0 131.1 jit_solution(17335974425128062268)
XLA Ops:
  6.5 0.0 all-gather.4.cloned.1.call-start
  6.5 0.7 all-gather.4.cloned.1.call-update
  7.3 0.0 all-gather.6.cloned.1.call-start
  7.3 0.7 all-gather.6.cloned.1.call-update
  8.0 0.0 all-gather.8.cloned.1.call-start
  8.1 0.1 slice_bitcast_fusion
  8.1 4.9 %collective-permute-start = (s32[30]{0:T(128)S(1)}, s32[30]{0:T(128)S(1)}, u32[]{:S(2)}, u32[]{:S(2)}) collective-permute-start(s32[30]{0:T(128)S(1)} %slice_bitcast_fusion), channel_id=1, source_target_pairs={{0,4},{4,8},{8,12},{12,16},{16,20},{20,24},{24,28},{1,5},{5,9},{9,... | collective-permute-start | bytes 368 | tf_op jit(solution)/shard_map/ppermute | solution.py:12
  13.0 0.0 all-gather.8.cloned.1.call-update
  13.0 0.1 fusion.54
  13.2 1.1 collective-permute-done
  14.3 0.1 pad_add_fusion
  14.4 0.1 slice_compare_fusion
  14.4 0.1 iota_select_fusion
  14.5 0.3 reduce-window.9
  14.8 0.1 slice.278
  14.9 0.1 slice_reduce_fusion
  15.0 0.1 maximum_bitcast_fusion
  15.1 0.1 add_compare_fusion.20
  15.2 0.1 add_compare_fusion.11
  15.3 0.1 add_compare_fusion.29
  15.3 30.8 %all-gather.4.cloned.1.call-done = bf16[2048,1024]{1,0:T(8,128)(2,1)} async-done(((bf16[512,1024]{1,0:T(8,128)(2,1)}), bf16[2048,1024]{1,0:T(8,128)(2,1)}) %all-gather.4.cloned.1.call-update) | async-done | bytes 4194320 | tf_op jit(solution)/shard_map/all_gather | solution.py:38
  46.1 5.8 %fusion.12 = f32[1024,512]{0,1:T(8,128)} fusion(bf16[2048,1024]{1,0:T(8,128)(2,1)} %all-gather.4.cloned.1.call-done, bf16[1,512,2048]{2,1,0:T(8,128)(2,1)S(1)} %copy-done), kind=kOutput, calls=%fused_computation.44 | convolution fusion | flops 2147483648 | bytes 8388608 | tf_op jit(solution)/shard_map/rc,tr->ct/dot_general | solution.py:36
  52.0 30.2 %all-gather.6.cloned.1.call-done = bf16[2048,1024]{1,0:T(8,128)(2,1)} async-done(((bf16[512,1024]{1,0:T(8,128)(2,1)}), bf16[2048,1024]{1,0:T(8,128)(2,1)}) %all-gather.6.cloned.1.call-update) | async-done | bytes 4194320 | tf_op jit(solution)/shard_map/all_gather | solution.py:44
  82.2 5.4 %multiply_convert_fusion = bf16[1024,512]{0,1:T(8,128)(2,1)S(1)} fusion(f32[1024,512]{0,1:T(8,128)} %fusion.12, bf16[2048,1024]{1,0:T(8,128)(2,1)} %all-gather.6.cloned.1.call-done, bf16[1,512,2048]{2,1,0:T(8,128)(2,1)S(1)} %copy-done), kind=kOutput, calls=%fused_computation.49 | convolution fusion | flops 2150105088 | bytes 9437184 | tf_op jit(solution)/shard_map/rc,tr->ct/dot_general | solution.py:42
  87.6 3.4 %collective-permute-start.1 = (bf16[1024,30]{0,1:T(8,128)(2,1)S(1)}, bf16[1024,30]{0,1:T(8,128)(2,1)S(1)}, u32[]{:S(2)}, u32[]{:S(2)}) collective-permute-start(bf16[1024,30]{0,1:T(8,128)(2,1)S(1)} %slice.341), channel_id=1, source_target_pairs={{0,4},{4,8},{8,12},{12,16},{16,20},{20,24},{24,28},{1,5},{5,9},{9,... | collective-permute-start | bytes 184328 | tf_op jit(solution)/shard_map/ppermute | solution.py:12
  91.0 0.1 add_compare_fusion.2
  91.1 1.8 %collective-permute-done.1 = bf16[1024,30]{0,1:T(8,128)(2,1)S(1)} collective-permute-done((bf16[1024,30]{0,1:T(8,128)(2,1)S(1)}, bf16[1024,30]{0,1:T(8,128)(2,1)S(1)}, u32[]{:S(2)}, u32[]{:S(2)}) %collective-permute-start.1) | collective-permute-done | bytes 61472 | tf_op jit(solution)/shard_map/ppermute | solution.py:12
  92.9 15.9 %add_convert_fusion = bf16[1024,512]{0,1:T(8,128)(2,1)S(1)} fusion(bf16[1024,512]{0,1:T(8,128)(2,1)S(1)} %multiply_convert_fusion, bf16[1024,30]{0,1:T(8,128)(2,1)S(1)} %collective-permute-done.1, f32[1024]{0:T(1024)S(1)} %bitcast.79, f32[1024]{0:T(1024)S(1)} %bitcast.80, f32[1024]{0:T(1024)S(1)} %bitcast.51, f32[1024]{0:T(1024)S(1)} %bitcast.52, ...), kind=kLoop, calls=%fused_computation.48 | loop fusion | flops 112197632 | bytes 2305024 | tf_op jit(solution)/shard_map/convert_element_type | solution.py:53
  108.8 0.2 convert_reduce_fusion
  109.0 0.4 fusion.3
  109.5 8.8 %all-gather.8.cloned.1.call-done = bf16[1024,2048]{1,0:T(8,128)(2,1)} async-done(((bf16[1024,512]{1,0:T(8,128)(2,1)}), bf16[1024,2048]{1,0:T(8,128)(2,1)}) %all-gather.8.cloned.1.call-update) | async-done | bytes 4194320 | tf_op jit(solution)/shard_map/all_gather | solution.py:62
  118.2 6.3 %fusion = bf16[1,512,2048]{2,1,0:T(8,128)(2,1)} fusion(bf16[1024,2048]{1,0:T(8,128)(2,1)} %all-gather.8.cloned.1.call-done, bf16[1024,512]{0,1:T(8,128)(2,1)S(1)} %add_convert_fusion, f32[1024]{0:T(1024)S(1)} %copy-done.4, f32[1024]{0:T(1024)S(1)} %copy-done.5, f32[512]{0:T(512)S(1)} %add_rsqrt_fusion, f32[512]{0:T(512)S(1)} %broadcast_multiply_fusion), kind=kOutput, calls=%fused_computation.30 | convolution fusion | flops 2153775104 | bytes 7352320 | tf_op jit(solution)/shard_map/ct,cr->tr/dot_general | solution.py:59
  (19 shorter events, 0.1 us)
Async XLA Ops:
  6.5 39.6 %copy-start = (bf16[1,512,2048]{2,1,0:T(8,128)(2,1)S(1)}, bf16[1,512,2048]{2,1,0:T(8,128)(2,1)}, u32[]{:S(2)}) copy-start(bf16[1,512,2048]{2,1,0:T(8,128)(2,1)} %param.9) | copy-start | bytes 6291460
  6.5 1.5 %copy-start.3 = (s32[1,512]{1,0:T(1,128)S(1)}, s32[1,512]{1,0:T(1,128)}, u32[]{:S(2)}) copy-start(s32[1,512]{1,0:T(1,128)} %param.10) | copy-start | bytes 6148
  6.5 6.5 %copy-start.1 = (f32[31,1024]{1,0:T(8,128)S(1)}, f32[31,1024]{1,0:T(8,128)}, u32[]{:S(2)}) copy-start(f32[31,1024]{1,0:T(8,128)} %param.14) | copy-start | bytes 380932
  6.5 39.6 %all-gather.4.cloned.1.call-start = ((), (), s32[]{:S(2)}) async-start(), calls=%async_computation | async-start | bytes 5242880 | tf_op jit(solution)/shard_map/all_gather | solution.py:38
  7.3 74.9 %all-gather.6.cloned.1.call-start = ((), (), s32[]{:S(2)}) async-start(), calls=%async_computation.1 | async-start | bytes 5242880 | tf_op jit(solution)/shard_map/all_gather | solution.py:44
  8.0 110.2 %all-gather.8.cloned.1.call-start = ((), (), s32[]{:S(2)}) async-start(), calls=%async_computation.2 | async-start | bytes 5242880 | tf_op jit(solution)/shard_map/all_gather | solution.py:62
  8.1 6.1 %collective-permute-start = (s32[30]{0:T(128)S(1)}, s32[30]{0:T(128)S(1)}, u32[]{:S(2)}, u32[]{:S(2)}) collective-permute-start(s32[30]{0:T(128)S(1)} %slice_bitcast_fusion), channel_id=1, source_target_pairs={{0,4},{4,8},{8,12},{12,16},{16,20},{20,24},{24,28},{1,5},{5,9},{9,... | collective-permute-start | bytes 368 | tf_op jit(solution)/shard_map/ppermute | solution.py:12
  52.0 40.9 %copy-start.2 = (f32[1024]{0:T(1024)S(1)}, f32[1024]{0:T(1024)}, u32[]{:S(2)}) copy-start(f32[1024]{0:T(1024)} %param.15) | copy-start | bytes 12292
  87.6 5.3 %collective-permute-start.1 = (bf16[1024,30]{0,1:T(8,128)(2,1)S(1)}, bf16[1024,30]{0,1:T(8,128)(2,1)S(1)}, u32[]{:S(2)}, u32[]{:S(2)}) collective-permute-start(bf16[1024,30]{0,1:T(8,128)(2,1)S(1)} %slice.341), channel_id=1, source_target_pairs={{0,4},{4,8},{8,12},{12,16},{16,20},{20,24},{24,28},{1,5},{5,9},{9,... | collective-permute-start | bytes 184328 | tf_op jit(solution)/shard_map/ppermute | solution.py:12
  92.9 25.3 %copy-start.4 = (f32[1024]{0:T(1024)S(1)}, f32[1024]{0:T(1024)}, u32[]{:S(2)}) copy-start(f32[1024]{0:T(1024)} %param.17) | copy-start | bytes 12292
  92.9 25.3 %copy-start.5 = (f32[1024]{0:T(1024)S(1)}, f32[1024]{0:T(1024)}, u32[]{:S(2)}) copy-start(f32[1024]{0:T(1024)} %param.16) | copy-start | bytes 12292
Sparse Core Ops, SparseCore 0:
  8.9 37.1 all-gather.3
  47.7 34.4 all-gather.5
  83.7 34.4 all-gather.7
where the time goes:
time: 131 us
  waiting for transfers between devices  74.1 us (57%)
  matrix products  17.6 us (13%)
  other arithmetic  17.5 us (13%)
  between operations  13.2 us (10%)
  starting transfers between devices  8.31 us (6%)
    all_gather x1, waiting for transfers between devices, body(): lax.all_gather(w_lin, 'dp', axis=0, tiled=True)  30.8 us
    all_gather x1, waiting for transfers between devices, body(): lax.all_gather(w_gate, 'dp', axis=0, tiled=True)  30.2 us
    convert_element_type x1, other arithmetic, body(): conved = lax.optimization_barrier(conv.astype(jnp.bfloat16))  15.9 us
    all_gather x1, waiting for transfers between devices, body(): lax.all_gather(w_out, 'dp', axis=1, tiled=True)  8.75 us
    ppermute x2, starting transfers between devices, from_behind(): return lax.ppermute(value, axis, pairs)  8.23 us
    dot_general x1, matrix products, body(): jnp.einsum('ct,cr->tr', act, lax.all_gather(w_out, 'dp', axis=1, tiled=Tr...  6.35 us
    dot_general x1, matrix products, body(): jnp.einsum('rc,tr->ct', lax.all_gather(w_lin, 'dp', axis=0, tiled=True),...  5.84 us
    dot_general x1, matrix products, body(): jnp.einsum('rc,tr->ct', lax.all_gather(w_gate, 'dp', axis=0, tiled=True),...  5.44 us
  transfers between devices with their start and end apart: 5, of which 5 were waited for; matrix products, arithmetic and copies ran while one was open for 22% of the time, Pallas kernels for 0%

commit v1 on v0

--- a/solution.py
+++ b/solution.py
@@ -1,9 +1,15 @@
+import functools
+
 import jax
 import jax.numpy as jnp
 from jax import lax
+from jax.experimental import pallas as pl
+from jax.experimental.pallas import tpu as pltpu
 from jax.sharding import PartitionSpec as P
 
-K = 31
+MESH = pl.DeviceIdType.MESH
+BLK = 256
+LANES = 128
 
 
 def from_behind(value, axis, by):
@@ -28,11 +34,11 @@
     return total
 
 
-def body(tokens, segments, w_lin, w_gate, w_out, conv_kernel, conv_bias, norm_gain, norm_bias):
+def plain_body(tokens, segments, w_lin, w_gate, w_out, conv_kernel, conv_bias, norm_gain, norm_bias):
     rows = tokens[0]
     doc_ids = segments[0]
     count = rows.shape[0]
-    reach = K - 1
+    reach = conv_kernel.shape[0] - 1
     first = jnp.einsum(
         "rc,tr->ct",
         lax.all_gather(w_lin, "dp", axis=0, tiled=True),
@@ -48,7 +54,8 @@
     glu = (first * jax.nn.sigmoid(second)).astype(jnp.bfloat16)
     tail, tail_ids = from_behind((glu[:, count - reach :], doc_ids[count - reach :]), "sp", 1)
     extended = jnp.concatenate([tail, glu], axis=1)
-    ext_ids = jnp.concatenate([tail_ids, doc_ids], axis=0)
+    first_block = lax.axis_index("sp") == 0
+    ext_ids = jnp.concatenate([jnp.where(first_block, -1, tail_ids), doc_ids], axis=0)
     conv = conv_doc(extended, ext_ids, conv_kernel, conv_bias)
     conved = lax.optimization_barrier(conv.astype(jnp.bfloat16))
     values = conved.astype(jnp.float32)
@@ -65,6 +72,325 @@
     return mixed_out[None]
 
 
+def kernel(
+    n_sp, n_dp, tok_hbm, seg_ref, lin_hbm, gate_hbm, wout_hbm, ck_ref, cb_ref, ng_ref, nb_ref,
+    out_ref,
+    tok, segh, segx, cnt, buf, glu, conv, act,
+    l_sem, h_send, h_recv, o_send, o_recv, y_send, y_recv, z_send, z_recv, x_send, x_recv,
+    c_send, c_recv,
+):
+    rows_, depth = tok_hbm.shape
+    shard = lin_hbm.shape[0]
+    width = lin_hbm.shape[1]
+    ocols = wout_hbm.shape[1]
+    taps = ck_ref.shape[0]
+    reach = taps - 1
+    halo = 32
+    full = rows_ + halo
+    chunks = width // BLK
+    hpb = shard // BLK
+    n_lg = 2 * chunks * hpb
+    n_wo = (width // BLK) * (ocols // BLK)
+    n_units = n_lg + n_wo
+    steps = n_units // 3
+    wo_base = 2 * chunks * depth
+
+    sp = lax.axis_index("sp")
+    dp = lax.axis_index("dp")
+    xb = lax.rem(sp, 2)
+    zb = lax.rem(sp // 2, 2)
+    x_dev = (sp + 1 - 2 * xb, dp)
+    z_dev = (sp + 2 - 4 * zb, dp)
+    ydp = lax.rem(dp + 2, n_dp)
+    y_dev = (sp, ydp)
+    c_dev = (sp, dp + 1 - 2 * lax.rem(dp, 2))
+    nxt = (lax.rem(sp + 1, n_sp), dp)
+    prv = (lax.rem(sp + n_sp - 1, n_sp), dp)
+    own_c = zb * 2 + (1 - zb) * xb
+    zrc_c = zb * xb + (1 - zb) * 2
+    xrc_c = 1 - xb
+
+    def lg_row(s, c, m, h):
+        return (2 * c + m) * depth + s * shard + h * BLK
+
+    def unit_row(s, u):
+        w = u // n_lg
+        lg = (u // hpb) * depth + s * shard + lax.rem(u, hpb) * BLK
+        wo = wo_base + s * n_wo * BLK + (u - n_lg) * BLK
+        return pl.multiple_of((1 - w) * lg + w * wo, BLK)
+
+    locals_ = []
+    for c in range(chunks):
+        for m, src in enumerate((lin_hbm, gate_hbm)):
+            row = pl.multiple_of(lg_row(dp, c, m, 0), BLK)
+            cp = pltpu.make_async_copy(
+                src.at[:, pl.ds(c * BLK, BLK)], buf.at[pl.ds(row, shard), :], l_sem.at[len(locals_)]
+            )
+            cp.start()
+            locals_.append((cp, row, shard))
+    for h in range(ocols // BLK):
+        row = pl.multiple_of(wo_base + dp * n_wo * BLK + h * width, BLK)
+        cp = pltpu.make_async_copy(
+            wout_hbm.at[:, pl.ds(h * BLK, BLK)], buf.at[pl.ds(row, width), :], l_sem.at[len(locals_)]
+        )
+        cp.start()
+        locals_.append((cp, row, width))
+    tcp = pltpu.make_async_copy(
+        tok_hbm, tok.at[pl.ds(halo, rows_), :], l_sem.at[len(locals_)]
+    )
+    tcp.start()
+
+    barrier = pltpu.get_barrier_semaphore()
+    for dev in (x_dev, z_dev, y_dev, c_dev, nxt, prv):
+        pl.semaphore_signal(barrier, inc=1, device_id=dev, device_id_type=MESH)
+    pl.semaphore_wait(barrier, 6)
+
+    def rcopy(src, dst, ss, rs, dev):
+        return pltpu.make_async_remote_copy(
+            src_ref=src, dst_ref=dst, send_sem=ss, recv_sem=rs, device_id=dev, device_id_type=MESH
+        )
+
+    sends = []
+    seg_cp = rcopy(seg_ref.at[:, pl.ds(rows_ - LANES, LANES)], segh, h_send.at[1], h_recv.at[1], nxt)
+    seg_cp.start()
+    tok_cp = rcopy(
+        tok_hbm.at[pl.ds(rows_ - halo, halo), :], tok.at[pl.ds(0, halo), :], h_send.at[0], h_recv.at[0], nxt
+    )
+    tok_cp.start()
+    sends += [seg_cp, tok_cp]
+
+    def ucopy(s, u, ss, rs, dev):
+        row = unit_row(s, u)
+        ref = buf.at[pl.ds(row, BLK), :]
+        return rcopy(ref, ref, ss, rs, dev)
+
+    ydone = 0
+    owns = []
+    for n, (cp, row, size) in enumerate(locals_):
+        cp.wait()
+        if n < 2 * chunks:
+            have = (n + 1) * hpb
+        else:
+            have = n_lg + (n + 1 - 2 * chunks) * (width // BLK)
+        while ydone < steps and 3 * ydone + 2 < have:
+            yc = ucopy(dp, 3 * ydone + own_c, y_send.at[ydone], y_recv.at[ydone], y_dev)
+            yc.start()
+            sends.append(yc)
+            ydone += 1
+        ref = buf.at[pl.ds(row, size), :]
+        oc = rcopy(ref, ref, o_send.at[n], o_recv.at[n], c_dev)
+        oc.start()
+        sends.append(oc)
+        owns.append(oc)
+
+    def forward(i, kind, color):
+        cc = ucopy(ydp, 3 * i + color, c_send.at[3 * i + kind], c_recv.at[3 * i + kind], c_dev)
+        cc.start()
+        sends.append(cc)
+
+    fwd = {}
+
+    def y_copy(i):
+        return ucopy(dp, 3 * i + own_c, y_send.at[i], y_recv.at[i], y_dev)
+
+    def stage_y(i):
+        ucopy(ydp, 3 * i + own_c, y_send.at[i], y_recv.at[i], y_dev).wait_recv()
+        zc = ucopy(ydp, 3 * i + own_c, z_send.at[i], z_recv.at[i], z_dev)
+        zc.start()
+        xc = ucopy(ydp, 3 * i + xb, x_send.at[i], x_recv.at[i], x_dev)
+
+        @pl.when(zb == 0)
+        def _():
+            xc.start()
+
+        sends.append(zc)
+        sends.append(xc)
+        forward(i, 0, own_c)
+
+    def stage_z(i):
+        ucopy(ydp, 3 * i + zrc_c, z_send.at[i], z_recv.at[i], z_dev).wait_recv()
+        xc = ucopy(ydp, 3 * i + xb, x_send.at[i], x_recv.at[i], x_dev)
+
+        @pl.when(zb == 1)
+        def _():
+            xc.start()
+
+        forward(i, 1, zrc_c)
+
+    def stage_x(i):
+        ucopy(ydp, 3 * i + xrc_c, x_send.at[i], x_recv.at[i], x_dev).wait_recv()
+        forward(i, 2, xrc_c)
+
+    cdp = ydp + 1 - 2 * lax.rem(ydp, 2)
+    waited = set()
+
+    def core_wait(i):
+        if i in waited:
+            return
+        waited.add(i)
+        for kind, color in enumerate((own_c, zrc_c, xrc_c)):
+            ucopy(cdp, 3 * i + color, c_send.at[3 * i + kind], c_recv.at[3 * i + kind], c_dev).wait_recv()
+
+    def tick(n):
+        if 0 <= n < steps:
+            stage_y(n)
+        if 0 <= n - 2 < steps:
+            stage_z(n - 2)
+        if 0 <= n - 3 < steps:
+            stage_x(n - 3)
+
+    def count_rows():
+        seg_cp.wait_recv()
+        before = jnp.where(sp == 0, -1, segh[...])[:, LANES - halo :]
+        line = jnp.concatenate([before, seg_ref[...]], axis=1)
+        pad = 640 - full
+        line = jnp.concatenate([line, jnp.zeros((1, pad), jnp.int32)], axis=1) if pad else line
+        tall = jnp.transpose(jnp.broadcast_to(line, (LANES, line.shape[1])))
+        segx[...] = tall[:full]
+
+        def one(r, carry):
+            base = pl.multiple_of(r * 64, 64)
+            here = segx[pl.ds(base + halo, 64), :]
+            total = jnp.zeros((64, LANES), jnp.int32)
+            for k in range(1, taps):
+                total = total + (segx[pl.ds(base + halo - k, 64), :] == here).astype(jnp.int32)
+            cnt[pl.ds(base, 64), :] = total
+            return carry
+
+        lax.fori_loop(0, rows_ // 64, one, 0)
+
+    def project(c):
+        for m in range(2):
+            owns[2 * c + m].wait_recv()
+        lin = jnp.dot(
+            tok[...], buf[pl.ds(2 * c * depth, depth), :], preferred_element_type=jnp.float32
+        )
+        gate = jnp.dot(
+            tok[...], buf[pl.ds((2 * c + 1) * depth, depth), :], preferred_element_type=jnp.float32
+        )
+        val = (lin * (1.0 / (1.0 + jnp.exp(-gate)))).astype(jnp.bfloat16).astype(jnp.float32)
+        for h in range(BLK // LANES):
+            glu[c * (BLK // LANES) + h] = val[:, h * LANES : (h + 1) * LANES]
+
+    RT = 64
+
+    def convolve(c):
+        for h in range(BLK // LANES):
+            g = c * (BLK // LANES) + h
+            lanes = pl.ds(g * LANES, LANES)
+
+            def one(r, carry):
+                base = pl.multiple_of(r * RT, RT)
+                valid = cnt[pl.ds(base, RT), :]
+                total = cb_ref[:, lanes] + ck_ref[pl.ds(reach, 1), lanes] * glu[g, pl.ds(base + halo, RT), :]
+                for k in range(1, taps):
+                    piece = glu[g, pl.ds(base + halo - k, RT), :]
+                    total = total + ck_ref[pl.ds(reach - k, 1), lanes] * jnp.where(valid >= k, piece, 0.0)
+                conv[pl.ds(base, RT), lanes] = total.astype(jnp.bfloat16)
+                return carry
+
+            lax.fori_loop(0, rows_ // RT, one, 0)
+
+    def normalise():
+        def one(r, carry):
+            base = pl.multiple_of(r * 32, 32)
+            v = conv[pl.ds(base, 32), :].astype(jnp.float32)
+            mean = jnp.mean(v, axis=1, keepdims=True)
+            dev = v - mean
+            var = jnp.mean(dev * dev, axis=1, keepdims=True)
+            nrm = dev * lax.rsqrt(var + 1e-05) * ng_ref[...] + nb_ref[...]
+            act[pl.ds(base, 32), :] = (nrm / (1.0 + jnp.exp(-nrm))).astype(jnp.bfloat16)
+            return carry
+
+        lax.fori_loop(0, rows_ // 32, one, 0)
+
+    def emit(s, h):
+        row = wo_base + s * n_wo * BLK + h * width
+        out_ref[:, pl.ds(s * ocols + h * BLK, BLK)] = jnp.dot(
+            act[...], buf[pl.ds(row, width), :], preferred_element_type=jnp.float32
+        ).astype(jnp.bfloat16)
+
+    ready = 0
+    tick(0)
+    count_rows()
+    tcp.wait()
+    tok_cp.wait_recv()
+    at = 1
+    for c in range(chunks):
+        need = (2 * hpb * (c + 1) - 1) // 3
+        while at <= need + 3:
+            tick(at)
+            at += 1
+        for i in range(ready, need + 1):
+            core_wait(i)
+        ready = need + 1
+        project(c)
+        tick(at)
+        at += 1
+        convolve(c)
+    while at <= steps + 2:
+        tick(at)
+        at += 1
+    normalise()
+    for i in range(ready, steps):
+        core_wait(i)
+    for h in range(ocols // BLK):
+        owns[2 * chunks + h].wait_recv()
+    for s in range(n_dp):
+        for h in range(ocols // BLK):
+            emit(s, h)
+    for cp in sends:
+        cp.wait_send()
+
+
+def fast_body(n_sp, n_dp, tokens, segments, w_lin, w_gate, w_out, conv_kernel, conv_bias, norm_gain, norm_bias):
+    rows, depth = tokens.shape[1:]
+    width = w_lin.shape[1]
+    ocols = w_out.shape[1]
+    units = (2 * w_lin.shape[0] * width + width * ocols) // (BLK * BLK)
+    steps = units // 3
+    n_local = 2 * (width // BLK) + ocols // BLK
+    vm = pl.BlockSpec(memory_space=pltpu.VMEM)
+    hb = pl.BlockSpec(memory_space=pl.ANY)
+    dma = pltpu.SemaphoreType.DMA
+    out = pl.pallas_call(
+        functools.partial(kernel, n_sp, n_dp),
+        out_shape=jax.ShapeDtypeStruct((rows, ocols * n_dp), jnp.bfloat16),
+        in_specs=[hb, vm, hb, hb, hb, vm, vm, vm, vm],
+        out_specs=vm,
+        scratch_shapes=[
+            pltpu.VMEM((rows + 32, depth), jnp.bfloat16),
+            pltpu.VMEM((1, LANES), jnp.int32),
+            pltpu.VMEM((rows + 32, LANES), jnp.int32),
+            pltpu.VMEM((rows, LANES), jnp.int32),
+            pltpu.VMEM((units * n_dp * BLK, BLK), jnp.bfloat16),
+            pltpu.VMEM((width // LANES, rows + 32, LANES), jnp.float32),
+            pltpu.VMEM((rows, width), jnp.bfloat16),
+            pltpu.VMEM((rows, width), jnp.bfloat16),
+            dma((n_local + 1,)),
+            dma((2,)),
+            dma((2,)),
+            dma((n_local,)),
+            dma((n_local,)),
+            dma((steps,)),
+            dma((steps,)),
+            dma((steps,)),
+            dma((steps,)),
+            dma((steps,)),
+            dma((steps,)),
+            dma((steps * 3,)),
+            dma((steps * 3,)),
+        ],
+        compiler_params=pltpu.CompilerParams(
+            collective_id=0, has_side_effects=True, vmem_limit_bytes=60 * 1024 * 1024
+        ),
+    )(
+        tokens[0], segments, w_lin, w_gate, w_out, conv_kernel,
+        conv_bias[None], norm_gain[None], norm_bias[None],
+    )
+    return out[None]
+
+
 def solution(mesh):
     placed = (
         P("dp", "sp", None),
@@ -77,6 +403,8 @@
         P(),
         P(),
     )
+    n_sp, n_dp = mesh.shape["sp"], mesh.shape["dp"]
+    body = functools.partial(fast_body, n_sp, n_dp) if n_dp == 4 and n_sp % 4 == 0 else plain_body
     return jax.shard_map(
         body, mesh=mesh, in_specs=placed, out_specs=P("dp", "sp", None), check_vma=False
     )

time: 131 us -> 58.3 us (0.45)
  the two profiles are of different devices: /device:TPU:0 before, /device:TPU:9 now
where the time goes in v1:
time: 58.3 us; the launch traced here: 58.1 us
  Pallas kernels  54.9 us (94%)
  local copies, waits for them, and re-layouts  3.16 us (5%)
    pallas_call x1, Pallas kernels, fast_body(): pl.pallas_call(functools.partial(kernel, n_sp, n_dp), out_shape=jax.Shape...  54.9 us
    unnamed x1, local copies, waits for them, and re-layouts  3.16 us

profile of v1, /device:TPU:9, one launch (start us, length us, event | category | flops | bytes accessed | tf_op | source)
XLA Modules:
  0.0 58.1 jit_solution(17853310701242844139)
XLA Ops:
  0.0 54.9 %shard_map.91 = bf16[512,2048]{1,0:T(8,128)(2,1)} custom-call(bf16[512,2048]{1,0:T(8,128)(2,1)} %bitcast.6, s32[1,512]{1,0:T(1,128)} %seg_ref.1, bf16[512,1024]{1,0:T(8,128)(2,1)} %lin_hbm.1, bf16[512,1024]{1,0:T(8,128)(2,1)} %gate_hbm.1, bf16[1024,512]{1,0:T(8,128)(2,1)} %wout_hbm.1, f32[31,1024]{1,0:T(8,128)} %ck_ref.1, f32[1,1024]{1,0:T(1,128)} %bitcast.7, ...), custom_call_target="tpu_custom_call" | custom-call | tf_op jit(solution)/shard_map/pallas_call | solution.py:356
  55.0 3.2 %copy.11 = bf16[1,512,2048]{2,1,0:T(8,128)(2,1)} copy(bf16[1,512,2048]{2,1,0:T(8,128)(2,1)} %bitcast.5) | data formatting | bytes 4194304

commit v2 on v1

--- a/solution.py
+++ b/solution.py
@@ -10,6 +10,12 @@
 MESH = pl.DeviceIdType.MESH
 BLK = 256
 LANES = 128
+UB = 128
+VMEM_MAX = 67043328
+SPARE = 512 * 1024
+RT = 64
+SKEW_Z = 3
+SKEW_X = 6
 
 
 def from_behind(value, axis, by):
@@ -88,9 +94,9 @@
     halo = 32
     full = rows_ + halo
     chunks = width // BLK
-    hpb = shard // BLK
+    hpb = shard // UB
     n_lg = 2 * chunks * hpb
-    n_wo = (width // BLK) * (ocols // BLK)
+    n_wo = (width // UB) * (ocols // BLK)
     n_units = n_lg + n_wo
     steps = n_units // 3
     wo_base = 2 * chunks * depth
@@ -110,26 +116,26 @@
     zrc_c = zb * xb + (1 - zb) * 2
     xrc_c = 1 - xb
 
-    def lg_row(s, c, m, h):
-        return (2 * c + m) * depth + s * shard + h * BLK
+    def lg_row(s, c, m):
+        return (2 * c + m) * depth + s * shard
 
     def unit_row(s, u):
         w = u // n_lg
-        lg = (u // hpb) * depth + s * shard + lax.rem(u, hpb) * BLK
-        wo = wo_base + s * n_wo * BLK + (u - n_lg) * BLK
-        return pl.multiple_of((1 - w) * lg + w * wo, BLK)
+        lg = (u // hpb) * depth + s * shard + lax.rem(u, hpb) * UB
+        wo = wo_base + s * n_wo * UB + (u - n_lg) * UB
+        return pl.multiple_of((1 - w) * lg + w * wo, UB)
 
     locals_ = []
     for c in range(chunks):
         for m, src in enumerate((lin_hbm, gate_hbm)):
-            row = pl.multiple_of(lg_row(dp, c, m, 0), BLK)
+            row = pl.multiple_of(lg_row(dp, c, m), UB)
             cp = pltpu.make_async_copy(
                 src.at[:, pl.ds(c * BLK, BLK)], buf.at[pl.ds(row, shard), :], l_sem.at[len(locals_)]
             )
             cp.start()
             locals_.append((cp, row, shard))
     for h in range(ocols // BLK):
-        row = pl.multiple_of(wo_base + dp * n_wo * BLK + h * width, BLK)
+        row = pl.multiple_of(wo_base + dp * n_wo * UB + h * width, UB)
         cp = pltpu.make_async_copy(
             wout_hbm.at[:, pl.ds(h * BLK, BLK)], buf.at[pl.ds(row, width), :], l_sem.at[len(locals_)]
         )
@@ -161,7 +167,7 @@
 
     def ucopy(s, u, ss, rs, dev):
         row = unit_row(s, u)
-        ref = buf.at[pl.ds(row, BLK), :]
+        ref = buf.at[pl.ds(row, UB), :]
         return rcopy(ref, ref, ss, rs, dev)
 
     ydone = 0
@@ -171,7 +177,7 @@
         if n < 2 * chunks:
             have = (n + 1) * hpb
         else:
-            have = n_lg + (n + 1 - 2 * chunks) * (width // BLK)
+            have = n_lg + (n + 1 - 2 * chunks) * (width // UB)
         while ydone < steps and 3 * ydone + 2 < have:
             yc = ucopy(dp, 3 * ydone + own_c, y_send.at[ydone], y_recv.at[ydone], y_dev)
             yc.start()
@@ -234,10 +240,10 @@
     def tick(n):
         if 0 <= n < steps:
             stage_y(n)
-        if 0 <= n - 2 < steps:
-            stage_z(n - 2)
-        if 0 <= n - 3 < steps:
-            stage_x(n - 3)
+        if 0 <= n - SKEW_Z < steps:
+            stage_z(n - SKEW_Z)
+        if 0 <= n - SKEW_X < steps:
+            stage_x(n - SKEW_X)
 
     def count_rows():
         seg_cp.wait_recv()
@@ -268,77 +274,96 @@
         gate = jnp.dot(
             tok[...], buf[pl.ds((2 * c + 1) * depth, depth), :], preferred_element_type=jnp.float32
         )
-        val = (lin * (1.0 / (1.0 + jnp.exp(-gate)))).astype(jnp.bfloat16).astype(jnp.float32)
+        val = (lin * (0.5 + 0.5 * jnp.tanh(0.5 * gate))).astype(jnp.bfloat16).astype(jnp.float32)
         for h in range(BLK // LANES):
             glu[c * (BLK // LANES) + h] = val[:, h * LANES : (h + 1) * LANES]
 
-    RT = 64
-
-    def convolve(c):
-        for h in range(BLK // LANES):
-            g = c * (BLK // LANES) + h
-            lanes = pl.ds(g * LANES, LANES)
-
-            def one(r, carry):
-                base = pl.multiple_of(r * RT, RT)
-                valid = cnt[pl.ds(base, RT), :]
-                total = cb_ref[:, lanes] + ck_ref[pl.ds(reach, 1), lanes] * glu[g, pl.ds(base + halo, RT), :]
-                for k in range(1, taps):
-                    piece = glu[g, pl.ds(base + halo - k, RT), :]
-                    total = total + ck_ref[pl.ds(reach - k, 1), lanes] * jnp.where(valid >= k, piece, 0.0)
-                conv[pl.ds(base, RT), lanes] = total.astype(jnp.bfloat16)
-                return carry
-
-            lax.fori_loop(0, rows_ // RT, one, 0)
-
-    def normalise():
+    def convolve(c, part, parts):
+        groups = [c * (BLK // LANES) + h for h in range(BLK // LANES)]
+
         def one(r, carry):
-            base = pl.multiple_of(r * 32, 32)
+            base = pl.multiple_of(part * (rows_ // parts) + r * RT, RT)
+            valid = cnt[pl.ds(base, RT), :]
+            lanes = [pl.ds(g * LANES, LANES) for g in groups]
+            totals = [
+                cb_ref[:, ln] + ck_ref[pl.ds(reach, 1), ln] * glu[g, pl.ds(base + halo, RT), :]
+                for g, ln in zip(groups, lanes)
+            ]
+            for k in range(1, taps):
+                keep = valid >= k
+                for n, (g, ln) in enumerate(zip(groups, lanes)):
+                    piece = jnp.where(keep, glu[g, pl.ds(base + halo - k, RT), :], 0.0)
+                    totals[n] = totals[n] + ck_ref[pl.ds(reach - k, 1), ln] * piece
+            for ln, total in zip(lanes, totals):
+                conv[pl.ds(base, RT), ln] = total.astype(jnp.bfloat16)
+            return carry
+
+        lax.fori_loop(0, rows_ // parts // RT, one, 0)
+
+    def normalise(part, parts):
+        each = rows_ // parts // 32
+
+        def one(r, carry):
+            base = pl.multiple_of(part * (rows_ // parts) + r * 32, 32)
             v = conv[pl.ds(base, 32), :].astype(jnp.float32)
             mean = jnp.mean(v, axis=1, keepdims=True)
             dev = v - mean
             var = jnp.mean(dev * dev, axis=1, keepdims=True)
             nrm = dev * lax.rsqrt(var + 1e-05) * ng_ref[...] + nb_ref[...]
-            act[pl.ds(base, 32), :] = (nrm / (1.0 + jnp.exp(-nrm))).astype(jnp.bfloat16)
+            act[pl.ds(base, 32), :] = (nrm * (0.5 + 0.5 * jnp.tanh(0.5 * nrm))).astype(jnp.bfloat16)
             return carry
 
-        lax.fori_loop(0, rows_ // 32, one, 0)
+        lax.fori_loop(0, each, one, 0, unroll=2)
 
     def emit(s, h):
-        row = wo_base + s * n_wo * BLK + h * width
-        out_ref[:, pl.ds(s * ocols + h * BLK, BLK)] = jnp.dot(
+        row = pl.multiple_of(wo_base + s * n_wo * UB + h * width, UB)
+        at_col = pl.multiple_of(s * ocols + h * BLK, BLK)
+        out_ref[:, pl.ds(at_col, BLK)] = jnp.dot(
             act[...], buf[pl.ds(row, width), :], preferred_element_type=jnp.float32
         ).astype(jnp.bfloat16)
 
-    ready = 0
-    tick(0)
+    state = {"at": 0, "ready": 0}
+
+    def advance(upto=None):
+        goal = state["at"] if upto is None else upto
+        while state["at"] <= min(goal, steps - 1 + SKEW_X):
+            tick(state["at"])
+            state["at"] += 1
+
+    def all_from_core(need):
+        for i in range(state["ready"], need + 1):
+            core_wait(i)
+        state["ready"] = max(state["ready"], need + 1)
+
+    advance(0)
     count_rows()
     tcp.wait()
     tok_cp.wait_recv()
-    at = 1
     for c in range(chunks):
         need = (2 * hpb * (c + 1) - 1) // 3
-        while at <= need + 3:
-            tick(at)
-            at += 1
-        for i in range(ready, need + 1):
-            core_wait(i)
-        ready = need + 1
+        advance(need + SKEW_X)
+        all_from_core(need)
         project(c)
-        tick(at)
-        at += 1
-        convolve(c)
-    while at <= steps + 2:
-        tick(at)
-        at += 1
-    normalise()
-    for i in range(ready, steps):
-        core_wait(i)
-    for h in range(ocols // BLK):
+        advance()
+        for h in range(2):
+            convolve(c, h, 2)
+            advance()
+    normalise(0, 2)
+    advance()
+    normalise(1, 2)
+    advance()
+    heads = ocols // BLK
+    for h in range(heads):
         owns[2 * chunks + h].wait_recv()
-    for s in range(n_dp):
-        for h in range(ocols // BLK):
-            emit(s, h)
+        emit(dp, h)
+        emit(dp + 1 - 2 * lax.rem(dp, 2), h)
+        advance()
+    for h in range(heads):
+        need = (n_lg + (h + 1) * (width // UB) - 1) // 3
+        advance(need + SKEW_X)
+        emit(ydp, h)
+        all_from_core(need)
+        emit(cdp, h)
     for cp in sends:
         cp.wait_send()
 
@@ -347,15 +372,15 @@
     rows, depth = tokens.shape[1:]
     width = w_lin.shape[1]
     ocols = w_out.shape[1]
-    units = (2 * w_lin.shape[0] * width + width * ocols) // (BLK * BLK)
+    units = (2 * w_lin.shape[0] * width + width * ocols) // (BLK * UB)
     steps = units // 3
     n_local = 2 * (width // BLK) + ocols // BLK
     vm = pl.BlockSpec(memory_space=pltpu.VMEM)
-    hb = pl.BlockSpec(memory_space=pl.ANY)
+    hb = pl.BlockSpec(memory_space=pltpu.HBM)
     dma = pltpu.SemaphoreType.DMA
     out = pl.pallas_call(
         functools.partial(kernel, n_sp, n_dp),
-        out_shape=jax.ShapeDtypeStruct((rows, ocols * n_dp), jnp.bfloat16),
+        out_shape=pltpu.VMEM((rows, ocols * n_dp), jnp.bfloat16),
         in_specs=[hb, vm, hb, hb, hb, vm, vm, vm, vm],
         out_specs=vm,
         scratch_shapes=[
@@ -363,7 +388,7 @@
             pltpu.VMEM((1, LANES), jnp.int32),
             pltpu.VMEM((rows + 32, LANES), jnp.int32),
             pltpu.VMEM((rows, LANES), jnp.int32),
-            pltpu.VMEM((units * n_dp * BLK, BLK), jnp.bfloat16),
+            pltpu.VMEM((units * n_dp * UB, BLK), jnp.bfloat16),
             pltpu.VMEM((width // LANES, rows + 32, LANES), jnp.float32),
             pltpu.VMEM((rows, width), jnp.bfloat16),
             pltpu.VMEM((rows, width), jnp.bfloat16),
@@ -382,7 +407,7 @@
             dma((steps * 3,)),
         ],
         compiler_params=pltpu.CompilerParams(
-            collective_id=0, has_side_effects=True, vmem_limit_bytes=60 * 1024 * 1024
+            collective_id=0, has_side_effects=True, vmem_limit_bytes=VMEM_MAX - rows * ocols * n_dp * 2 - SPARE
         ),
     )(
         tokens[0], segments, w_lin, w_gate, w_out, conv_kernel,

time: 58.3 us -> 48.8 us (0.84)
  the two profiles are of different devices: /device:TPU:9 before, /device:TPU:0 now
where the time goes in v2:
time: 48.8 us; the launch traced here: 48.7 us
  Pallas kernels  47.3 us (97%)
  local copies, waits for them, and re-layouts  1.32 us (3%)
    pallas_call x1, Pallas kernels, fast_body(): pl.pallas_call(functools.partial(kernel, n_sp, n_dp), out_shape=pltpu.VME...  47.3 us
    unnamed x1, local copies, waits for them, and re-layouts  1.32 us

profile of v2, /device:TPU:0, one launch (start us, length us, event | category | flops | bytes accessed | tf_op | source)
XLA Modules:
  0.0 48.7 jit_solution(17451987058741931399)
XLA Ops:
  0.0 47.3 %shard_map.91 = bf16[512,2048]{1,0:T(8,128)(2,1)S(1)} custom-call(bf16[512,2048]{1,0:T(8,128)(2,1)} %bitcast.6, s32[1,512]{1,0:T(1,128)} %seg_ref.1, bf16[512,1024]{1,0:T(8,128)(2,1)} %lin_hbm.1, bf16[512,1024]{1,0:T(8,128)(2,1)} %gate_hbm.1, bf16[1024,512]{1,0:T(8,128)(2,1)} %wout_hbm.1, f32[31,1024]{1,0:T(8,128)} %ck_ref.1, f32[1,1024]{1,0:T(1,128)} %bitcast.7, ...), custom_call_target="tpu_custom_call" | custom-call | tf_op jit(solution)/shard_map/pallas_call | solution.py:381
  47.3 1.3 %copy.11 = bf16[1,512,2048]{2,1,0:T(8,128)(2,1)} copy(bf16[1,512,2048]{2,1,0:T(8,128)(2,1)S(1)} %bitcast.5) | data formatting | bytes 4194304
